TPU v7x, 512 devices: a 4x2x32 block of a 4x8x32 slice. The times are simulated.
512 devices in a mesh: grp: 2 (over y), sp: 64 (over z, core), tp: 4 (over x).
Axes of the slice: x: 4, y: 2, z: 32, core: 2. Of those that a mesh axis runs over, the one named last changes fastest.
The devices are a block of a 4x8x32 slice.
Arguments:
- tokens: bfloat16 [20480, 2048], P(('grp', 'sp')), parts along dimension 0, may hold values from -6 to 6
- norm_gain: float32 [2048], replicated, may hold values from 0.6 to 5
- query_weight: bfloat16 [2048, 2048], P('sp', 'tp')
- key_weight: bfloat16 [2048, 512], P('sp', 'tp')
- value_weight: bfloat16 [2048, 512], P('sp', 'tp'), may hold values from -0.125 to 0.125
- map_lambda: float32 [16], P('tp'), may hold values from 0.3 to 0.8
- head_gain: float32 [16, 128], P('tp'), may hold values from 0.1 to 1.9
- attn_out_weight: bfloat16 [2048, 2048], P('tp', 'sp'), may hold values from -0.125 to 0.125
- pool_out_weight: bfloat16 [2048, 2048], P('tp', 'sp'), may hold values from -0.09375 to 0.09375
Outputs:
- mixed_rows: bfloat16 [20480, 2048], P(('grp', 'sp', 'tp')), parts along dimension 0
- log_totals: float32 [2, 16, 20480], P(None, 'tp', ('grp', 'sp')), parts along dimension 2
There are 2 independent parts, one for each index of `grp`. A program takes and returns all parts, laid end to end along the dimension named above; an argument that names none is the same for every part. Nothing has to cross between parts.
All inputs are finite; a program needn't handle non-finite values.
Results may differ from a plain program's by a relative error of at most 0.013.
The roundings to bfloat16 on the way count: a program that leaves them out, or rounds other values in their place, can miss the bound.
Values may be sent and summed in bfloat16 or wider, within the bound.
No kernel may reach another device: no remote copies, remote signals or barrier semaphores. Data moves between devices by JAX's collectives and lax.ppermute only.
A program may use at most 64 MiB of HBM per device.

v0:
```python
import math
import jax
import jax.numpy as jnp
from jax import lax
from jax.sharding import PartitionSpec as P

HD = 64
VD = 128
POOL_SPAN = 16
epsilon = 1e-06
very_low = -1e30


def extended(cells, sides, width):
    for axis, dim in sides:
        count = lax.axis_size(axis)
        ends = count - 1
        head = lax.slice_in_dim(cells, 0, width, axis=dim)
        tail = lax.slice_in_dim(cells, cells.shape[dim] - width, cells.shape[dim], axis=dim)
        cells = jnp.concatenate(
            [
                lax.ppermute(tail, axis, [(i, (i + 1) % count) for i in range(ends)]),
                cells,
                lax.ppermute(head, axis, [((i + 1) % count, i) for i in range(ends)]),
            ],
            axis=dim,
        )
    return cells


def side_by_side(arrays, axis, dim, along):
    both = jnp.concatenate(arrays, axis=along)
    whole, at, gathered = (lax.all_gather(both, axis, axis=dim, tiled=True), 0, [])
    for a in arrays:
        gathered.append(lax.slice_in_dim(whole, at, at + a.shape[along], axis=along))
        at += a.shape[along]
    return tuple(gathered)


def rows_first(arrays, axis, dims):
    turned = [jnp.moveaxis(a, dim, 0) for a, dim in zip(arrays, dims)]
    widths = [t[0].size for t in turned]
    both = jnp.concatenate([t.reshape(-1, w) for t, w in zip(turned, widths)], axis=1)
    whole = lax.all_gather(both, axis, axis=0, tiled=True)
    blocks = jnp.split(whole, [sum(widths[:k]) for k in range(1, len(widths))], axis=1)
    return tuple(
        (
            jnp.moveaxis(b.reshape(-1, *t.shape[1:]), 0, dim)
            for b, t, dim in zip(blocks, turned, dims)
        )
    )


def cut_along(x, dim, length):
    before, after = (x.shape[:dim], x.shape[dim + 1 :])
    return jnp.moveaxis(x.reshape(*before, length, -1, *after), dim, 0)


def sent_and_summed(x, axis, dim):
    blocks = cut_along(x, dim, lax.axis_size(axis))
    arrived = lax.all_to_all(blocks, axis, split_axis=0, concat_axis=0, tiled=True)
    return arrived.astype(jnp.float32).sum(axis=0)


def add_products(totals, pieces, source):
    results = []
    for running, piece in zip(totals, pieces):
        results.append(jnp.dot(source, piece, preferred_element_type=jnp.float32))
    return tuple(results)


def on_device(
    tokens,
    norm_gain,
    query_weight,
    key_weight,
    value_weight,
    map_lambda,
    head_gain,
    attn_out_weight,
    pool_out_weight,
):
    tokens_wide = tokens.astype(jnp.float32)
    normed = (
        tokens_wide
        * lax.rsqrt(jnp.mean(tokens_wide * tokens_wide, axis=-1, keepdims=True) + epsilon)
        * norm_gain
    ).astype(jnp.bfloat16)
    row_count = normed.shape[0]
    sp_index = lax.axis_index("sp")
    tp_index = lax.axis_index("tp")
    group_width = pool_out_weight.shape[0]
    local_heads = map_lambda.shape[0]
    key_heads = value_weight.shape[1] // VD
    group_heads = local_heads // key_heads
    q_empty = jnp.zeros((row_count, query_weight.shape[1]), jnp.float32)
    k_empty = jnp.zeros((row_count, key_weight.shape[1]), jnp.float32)
    v_empty = jnp.zeros((row_count, value_weight.shape[1]), jnp.float32)
    q_acc, k_acc, v_acc = add_products(
        (q_empty, k_empty, v_empty),
        side_by_side((query_weight, key_weight, value_weight), "sp", 0, 1),
        normed,
    )
    queries = q_acc.astype(jnp.bfloat16).reshape(row_count, key_heads, group_heads, 2, HD)
    keys_flat = k_acc.astype(jnp.bfloat16)
    values_flat = v_acc.astype(jnp.bfloat16)

    def key_block(state_now, key_pair):
        maxima, totals, accums = state_now
        key_blk, val_blk = key_pair
        scores = jnp.einsum(
            "qhgmd,khmd->hgmqk", queries, key_blk, preferred_element_type=jnp.float32
        ) * HD ** (-0.5)
        highest = jnp.maximum(maxima, jnp.max(scores, axis=-1))
        factor = jnp.exp(maxima - highest)
        weights = jnp.exp(scores - highest[..., None])
        totals = totals * factor + jnp.sum(weights, axis=-1)
        accums = accums * factor[..., None] + jnp.einsum(
            "hgmqk,khe->hgmqe",
            weights.astype(jnp.bfloat16),
            val_blk,
            preferred_element_type=jnp.float32,
        )
        return ((highest, totals, accums), None)

    start_state = (
        jnp.full((key_heads, group_heads, 2, row_count), very_low, jnp.float32),
        jnp.zeros((key_heads, group_heads, 2, row_count), jnp.float32),
        jnp.zeros((key_heads, group_heads, 2, row_count, VD), jnp.float32),
    )
    key_piece, val_piece = side_by_side((keys_flat, values_flat), "sp", 0, 1)
    piece_len = key_piece.shape[0]
    block_len = math.gcd(piece_len, 512)
    key_blocks = key_piece.reshape(piece_len // block_len, block_len, key_heads, 2, HD)
    val_blocks = val_piece.reshape(piece_len // block_len, block_len, key_heads, VD)
    state_next, unused = lax.scan(key_block, start_state, (key_blocks, val_blocks))
    maxima, totals, accums = state_next
    log_parts = maxima + jnp.log(totals)
    log_totals = jnp.transpose(log_parts, (2, 0, 1, 3)).reshape(2, local_heads, row_count)
    reads = accums / totals[..., None]
    contrast = reads[:, :, 0] - map_lambda.reshape(key_heads, group_heads, 1, 1) * reads[:, :, 1]
    scaled = (
        contrast
        * lax.rsqrt(jnp.mean(contrast * contrast, axis=-1, keepdims=True) + epsilon)
        * head_gain.reshape(key_heads, group_heads, 1, VD)
    )
    attention_head_rows = (
        jnp.transpose(scaled, (2, 0, 1, 3))
        .reshape(row_count, local_heads * VD)
        .astype(jnp.bfloat16)
    )
    head_rows, log_totals = (attention_head_rows, log_totals)
    own_chan = lax.dynamic_slice_in_dim(normed, tp_index * group_width, group_width, 1)
    reach = POOL_SPAN // 2
    padded = extended(own_chan, (("sp", 0),), reach)
    window = jnp.left_shift(jnp.int32(2), tp_index)
    half_span = window // 2
    running = jnp.zeros((row_count, group_width), jnp.float32)
    for offset in range(POOL_SPAN):
        piece = lax.dynamic_slice_in_dim(padded, reach - half_span + offset, row_count, 0).astype(
            jnp.float32
        )
        running = running + jnp.where(offset < window, piece, 0.0)
    seq_len = row_count * lax.axis_size("sp")
    position = sp_index * row_count + jnp.arange(row_count, dtype=jnp.int32)
    lower_edge = jnp.clip(position - half_span, 0, seq_len)
    upper_edge = jnp.clip(position + window - half_span, 0, seq_len)
    counts_f = (upper_edge - lower_edge).astype(jnp.float32)[:, None]
    pooled = (running / counts_f - own_chan.astype(jnp.float32)).astype(jnp.bfloat16)
    attn_whole, pool_whole = rows_first((attn_out_weight, pool_out_weight), "sp", (1, 1))
    mixed = sent_and_summed(
        (
            jnp.dot(head_rows, attn_whole, preferred_element_type=jnp.float32)
            + jnp.dot(pooled, pool_whole, preferred_element_type=jnp.float32)
        ).astype(jnp.bfloat16),
        "tp",
        0,
    )
    return (mixed.astype(jnp.bfloat16), log_totals)


def solution(mesh):
    placed = (
        P(("grp", "sp"), None),
        P(),
        P("sp", "tp"),
        P("sp", "tp"),
        P("sp", "tp"),
        P("tp"),
        P("tp", None),
        P("tp", "sp"),
        P("tp", "sp"),
    )
    return jax.shard_map(
        on_device,
        mesh=mesh,
        in_specs=placed,
        out_specs=(P(("grp", "sp", "tp"), None), P(None, "tp", ("grp", "sp"))),
        check_vma=False,
    )
```

profile of v0, /device:TPU:33, one launch (start us, length us, event | category | flops | bytes accessed | tf_op | source)
XLA Modules:
  0.0 463.9 jit_solution(1996531351021676169)
XLA Ops:
  11.4 161.0 %all-gather.4.cloned.1.call-done = bf16[2048,768]{1,0:T(8,128)(2,1)} async-done(((bf16[32,768]{1,0:T(8,128)(2,1)}), bf16[2048,768]{1,0:T(8,128)(2,1)}) %all-gather.4.cloned.1.call-update) | async-done | bytes 3145744 | tf_op jit(solution)/shard_map/all_gather | solution.py:33
  176.0 2.4 collective-permute-start
  178.4 2.0 collective-permute-start.1
  184.1 2.1 fusion.30
  186.4 118.8 %all-gather.6.cloned.1.call-done = bf16[10240,256]{1,0:T(8,128)(2,1)} async-done(((bf16[160,256]{1,0:T(8,128)(2,1)}), bf16[10240,256]{1,0:T(8,128)(2,1)}) %all-gather.6.cloned.1.call-update) | async-done | bytes 5242896 | tf_op jit(solution)/shard_map/all_gather | solution.py:33
  305.2 3.7 fusion.76
  308.9 4.2 reshape.146
  313.2 11.1 %copy.22 = bf16[20,512,1,2,64]{1,4,3,2,0:T(8,128)(2,1)} copy(bf16[20,512,1,2,64]{4,3,1,0,2:T(2,128)(2,1)} %reshape.146) | data formatting | bytes 5242880
  324.3 90.8 %while.15 = (s32[]{:T(128)}, f32[1,4,2,160]{3,1,2,0:T(4,128)S(1)}, f32[1,4,2,160]{3,1,2,0:T(4,128)}, f32[1,4,2,160,128]{4,3,2,1,0:T(8,128)S(1)}, bf16[20,512,1,2...) while((s32[]{:T(128)}, f32[1,4,2,160]{3,1,2,0:T(4,128)S(1)}, ...), condition=%wide.region_4.5_spmd.clone, body=%wide.region_1.4_spmd.clone.sunk | while | flops 256089600 | bytes 9730209 | solution.py:136
  324.3 1.6 bitcast_reduce_fusion.2
  328.8 1.6 bitcast_reduce_fusion.2
  333.4 1.6 bitcast_reduce_fusion.2
  337.9 1.6 bitcast_reduce_fusion.2
  342.5 1.6 bitcast_reduce_fusion.2
  347.0 1.6 bitcast_reduce_fusion.2
  351.6 1.6 bitcast_reduce_fusion.2
  356.1 1.6 bitcast_reduce_fusion.2
  360.7 1.6 bitcast_reduce_fusion.2
  365.2 1.6 bitcast_reduce_fusion.2
  369.7 1.6 bitcast_reduce_fusion.2
  374.3 1.6 bitcast_reduce_fusion.2
  378.8 1.6 bitcast_reduce_fusion.2
  383.4 1.6 bitcast_reduce_fusion.2
  387.9 1.6 bitcast_reduce_fusion.2
  397.0 1.6 bitcast_reduce_fusion.2
  401.5 1.6 bitcast_reduce_fusion.2
  406.1 1.6 bitcast_reduce_fusion.2
  418.1 17.0 %all-gather.8.cloned.1.call-done = bf16[2048,1024]{1,0:T(8,128)(2,1)} async-done(((bf16[32,1024]{1,0:T(8,128)(2,1)}), bf16[2048,1024]{1,0:T(8,128)(2,1)}) %all-gather.8.cloned.1.call-update) | async-done | bytes 4194320 | tf_op jit(solution)/shard_map/all_gather | solution.py:44
  435.1 2.4 fusion.23
  437.6 4.5 fusion.21
  442.1 4.1 all-to-all-start
  446.8 9.8 %all-to-all-done = bf16[4,40,2048]{2,1,0:T(8,128)(2,1)S(1)} async-done(((bf16[4,40,2048]{2,1,0:T(8,128)(2,1)}), bf16[4,40,2048]{2,1,0:T(8,128)(2,1)S(1)}, u32[]{:S(2)}, u32[]{:S(2)}) %all-to-all-start) | async-done | bytes 655392 | tf_op jit(solution)/shard_map/all_to_all | solution.py:61
  (249 shorter events, 75.9 us)
Async XLA Ops:
  7.2 173.2 %copy-start.7 = (bf16[512,32]{0,1:T(8,128)(2,1)S(1)}, bf16[512,32]{0,1:T(8,128)(2,1)}, u32[]{:S(2)}) copy-start(bf16[512,32]{0,1:T(8,128)(2,1)} %param.18) | copy-start | bytes 98308
  7.2 173.2 %copy-start.6 = (bf16[512,32]{0,1:T(8,128)(2,1)S(1)}, bf16[512,32]{0,1:T(8,128)(2,1)}, u32[]{:S(2)}) copy-start(bf16[512,32]{0,1:T(8,128)(2,1)} %param.19) | copy-start | bytes 98308
  7.2 165.2 %all-gather.4.cloned.1.call-start = ((), (), s32[]{:S(2)}) async-start(), calls=%async_computation.1 | async-start | bytes 3194880 | tf_op jit(solution)/shard_map/all_gather | solution.py:33
  8.7 296.4 %all-gather.6.cloned.1.call-start = ((), (), s32[]{:S(2)}) async-start(), calls=%async_computation.2 | async-start | bytes 5324800 | tf_op jit(solution)/shard_map/all_gather | solution.py:33
  175.9 259.2 %all-gather.8.cloned.1.call-start = ((), (), s32[]{:S(2)}) async-start(), calls=%async_computation.3 | async-start | bytes 4259840 | tf_op jit(solution)/shard_map/all_gather | solution.py:44
  176.0 5.8 %collective-permute-start = (bf16[8,512]{1,0:T(8,128)(2,1)S(1)}, bf16[8,512]{1,0:T(8,128)(2,1)S(1)}, u32[]{:S(2)}, u32[]{:S(2)}) collective-permute-start(bf16[8,512]{1,0:T(8,128)(2,1)S(1)} %get-tuple-element.104), channel_id=1, source_target_pairs={{0,4},{4,8},{8,12},{12,16},{16,20},{20,24},{24,28},{28,32},{32,36}... | collective-permute-start | bytes 24584 | tf_op jit(solution)/shard_map/ppermute | solution.py:22
  178.4 5.0 %collective-permute-start.1 = (bf16[8,512]{1,0:T(8,128)(2,1)S(1)}, bf16[8,512]{1,0:T(8,128)(2,1)S(1)}, u32[]{:S(2)}, u32[]{:S(2)}) collective-permute-start(bf16[8,512]{1,0:T(8,128)(2,1)S(1)} %get-tuple-element.105), channel_id=1, source_target_pairs={{4,0},{8,4},{12,8},{16,12},{20,16},{24,20},{28,24},{32,28},{36,32}... | collective-permute-start | bytes 24584 | tf_op jit(solution)/shard_map/ppermute | solution.py:24
  181.1 5.2 %copy-start = (bf16[160,512]{1,0:T(8,128)(2,1)}, bf16[160,512]{1,0:T(8,128)(2,1)S(1)}, u32[]{:S(2)}) copy-start(bf16[160,512]{1,0:T(8,128)(2,1)S(1)} %constant_dynamic-slice_fusion.1) | copy-start | bytes 491524
  326.0 2.2 copy-start.2
  330.5 2.3 copy-start.2
  335.1 2.2 copy-start.2
  339.6 2.3 copy-start.2
  344.1 2.2 copy-start.2
  348.7 2.3 copy-start.2
  353.2 2.3 copy-start.2
  357.8 2.3 copy-start.2
  362.3 2.2 copy-start.2
  371.4 2.2 copy-start.2
  375.9 2.2 copy-start.2
  380.5 2.2 copy-start.2
  385.0 2.3 copy-start.2
  389.6 2.3 copy-start.2
  394.1 2.2 copy-start.2
  398.6 2.3 copy-start.2
  403.2 2.2 copy-start.2
  407.7 2.2 copy-start.2
  412.3 2.3 copy-start.2
  416.1 21.4 %copy-start.1 = (bf16[160,512]{1,0:T(8,128)(2,1)S(1)}, bf16[160,512]{1,0:T(8,128)(2,1)}, u32[]{:S(2)}) copy-start(bf16[160,512]{1,0:T(8,128)(2,1)} %copy-done) | copy-start | bytes 491524
  416.1 21.4 %copy-start.5 = (bf16[176,512]{1,0:T(8,128)(2,1)S(1)}, bf16[176,512]{1,0:T(8,128)(2,1)}, u32[]{:S(2)}) copy-start(bf16[176,512]{1,0:T(8,128)(2,1)} %pad_maximum_fusion) | copy-start | bytes 540676
  416.1 21.4 %copy-start.8 = (f32[160]{0:T(256)S(1)}, f32[160]{0:T(256)}, u32[]{:S(2)}) copy-start(f32[160]{0:T(256)} %subtract_convert_fusion.2) | copy-start | bytes 1924
  437.5 8.7 %copy-start.4 = (f32[1,4,2,160]{3,1,2,0:T(4,128)S(1)}, f32[1,4,2,160]{3,1,2,0:T(4,128)}, u32[]{:S(2)}) copy-start(f32[1,4,2,160]{3,1,2,0:T(4,128)} %get-tuple-element.42) | copy-start | bytes 15364
  442.1 14.6 %all-to-all-start = ((bf16[4,40,2048]{2,1,0:T(8,128)(2,1)}), bf16[4,40,2048]{2,1,0:T(8,128)(2,1)S(1)}, u32[]{:S(2)}, u32[]{:S(2)}) async-start(bf16[4,40,2048]{2,1,0:T(8,128)(2,1)} %bitcast.9), calls=%async_computation | async-start | bytes 1310720 | tf_op jit(solution)/shard_map/all_to_all | solution.py:61
  (21 other events, 14.3 us)
Sparse Core Ops, SparseCore 0:
  10.7 161.6 all-gather.3
  176.0 129.1 all-gather.5
  307.3 127.7 all-gather.7
where the time goes:
time: 466 us; the launch traced here: 464 us
  waiting for transfers between devices  308 us (66%)
  matrix products  72.8 us (16%)
  local copies, waits for them, and re-layouts  32 us (7%)
  other arithmetic  26.8 us (6%)
  between operations  14 us (3%)
  starting transfers between devices  8.71 us (2%)
    all_gather x2, waiting for transfers between devices, side_by_side(): lax.all_gather(both, axis, axis=dim, tiled=True)  280 us
    dot_general x20, matrix products, key_block(): jnp.einsum('qhgmd,khmd->hgmqk', queries, key_blk, preferred_element_type=...  32.7 us
    dot_general x20, matrix products, key_block(): jnp.einsum('hgmqk,khe->hgmqe', weights.astype(jnp.bfloat16), val_blk, pre...  28.4 us
    all_gather x1, waiting for transfers between devices, rows_first(): whole = lax.all_gather(both, axis, axis=0, tiled=True)  17 us
    another operation x20, other arithmetic  16 us
    while x100, local copies, waits for them, and re-layouts  11.8 us
    unnamed x16, local copies, waits for them, and re-layouts  11.2 us
    all_to_all x1, waiting for transfers between devices, sent_and_summed(): lax.all_to_all(blocks, axis, split_axis=0, concat_axis=0, tiled=True)  9.8 us
  transfers between devices with their start and end apart: 6, of which 5 were waited for; matrix products, arithmetic and copies ran while one was open for 23% of the time, Pallas kernels for 0%

commit v1 on v0

--- a/solution.py
+++ b/solution.py
@@ -9,6 +9,19 @@
 POOL_SPAN = 16
 epsilon = 1e-06
 very_low = -1e30
+
+
+def arrange_column_over_axis(mesh_ax, packet):
+    step_out = jnp.concatenate(
+        lax.all_to_all(
+            jnp.stack([packet] * lax.axis_size(mesh_ax), axis=0),
+            axis_name=mesh_ax,
+            split_axis=0,
+            concat_axis=0,
+        ),
+        axis=0,
+    )
+    return step_out
 
 
 def extended(cells, sides, width):
@@ -41,7 +54,7 @@
     turned = [jnp.moveaxis(a, dim, 0) for a, dim in zip(arrays, dims)]
     widths = [t[0].size for t in turned]
     both = jnp.concatenate([t.reshape(-1, w) for t, w in zip(turned, widths)], axis=1)
-    whole = lax.all_gather(both, axis, axis=0, tiled=True)
+    whole = arrange_column_over_axis(axis, both)
     blocks = jnp.split(whole, [sum(widths[:k]) for k in range(1, len(widths))], axis=1)
     return tuple(
         (

time: 466 us -> 718 us (1.54)
  waiting for transfers between devices: 308 us -> 544 us
  starting transfers between devices: 8.71 us -> 23 us
    ppermute x1, waiting for transfers between devices: 0.01 us -> 356 us  [extended(): lax.ppermute(tail, axis, [(i, (i + 1) % count) for i in range(ends)])]
    all_gather x2, waiting for transfers between devices: 280 us -> 161 us  [side_by_side(): lax.all_gather(both, axis, axis=dim, tiled=True)]
    ppermute x1, waiting for transfers between devices: 1.63 us -> 19.5 us  [extended(): lax.ppermute(head, axis, [((i + 1) % count, i) for i in range(ends)])]
    all_gather x1 -> x0, waiting for transfers between devices: 17 us -> none  [rows_first(): whole = lax.all_gather(both, axis, axis=0, tiled=True)]
    all_to_all x0 -> x1, starting transfers between devices: none -> 13.8 us  [arrange_column_over_axis(): lax.all_to_all(jnp.stack([packet] * lax.axis_size(mesh_ax), axis=0), axis...]
  transfers between devices with their start and end apart: 6 -> 6, of which waited for: 5 -> 4; matrix products, arithmetic and copies ran while one was open for 23% -> 15% of each run, Pallas kernels for 0% -> 0%
where the time goes in v1:
time: 718 us; the launch traced here: 716 us
  waiting for transfers between devices  544 us (76%)
  matrix products  72.8 us (10%)
  local copies, waits for them, and re-layouts  34.7 us (5%)
  other arithmetic  26.1 us (4%)
  starting transfers between devices  23 us (3%)
  between operations  14.4 us (2%)
    ppermute x1, waiting for transfers between devices, extended(): lax.ppermute(tail, axis, [(i, (i + 1) % count) for i in range(ends)])  356 us
    all_gather x2, waiting for transfers between devices, side_by_side(): lax.all_gather(both, axis, axis=dim, tiled=True)  161 us
    dot_general x20, matrix products, key_block(): jnp.einsum('qhgmd,khmd->hgmqk', queries, key_blk, preferred_element_type=...  32.6 us
    dot_general x20, matrix products, key_block(): jnp.einsum('hgmqk,khe->hgmqe', weights.astype(jnp.bfloat16), val_blk, pre...  28.4 us
    ppermute x1, waiting for transfers between devices, extended(): lax.ppermute(head, axis, [((i + 1) % count, i) for i in range(ends)])  19.5 us
    another operation x20, other arithmetic  16 us
  transfers between devices with their start and end apart: 6, of which 4 were waited for; matrix products, arithmetic and copies ran while one was open for 15% of the time, Pallas kernels for 0%

profile of v1, /device:TPU:33, one launch (start us, length us, event | category | flops | bytes accessed | tf_op | source)
XLA Modules:
  0.0 715.9 jit_solution(3972975601754177202)
XLA Ops:
  11.4 161.0 %all-gather.3.cloned.1.call-done = bf16[2048,768]{1,0:T(8,128)(2,1)} async-done(((bf16[32,768]{1,0:T(8,128)(2,1)}), bf16[2048,768]{1,0:T(8,128)(2,1)}) %all-gather.3.cloned.1.call-update) | async-done | bytes 3145744 | tf_op jit(solution)/shard_map/all_gather | solution.py:46
  175.9 2.6 stack.2
  178.5 13.8 %all-to-all-start = ((bf16[64,32,1024]{2,1,0:T(8,128)(2,1)}), bf16[64,32,1024]{2,1,0:T(8,128)(2,1)}, u32[]{:S(2)}, u32[]{:S(2)}) async-start(bf16[64,32,1024]{2,1,0:T(8,128)(2,1)} %stack.2), calls=%async_computation | async-start | bytes 8388608 | tf_op jit(solution)/shard_map/all_to_all | solution.py:16
  192.4 3.6 collective-permute-start
  196.0 2.0 collective-permute-start.1
  198.6 355.9 %collective-permute-done = bf16[8,512]{1,0:T(8,128)(2,1)S(1)} collective-permute-done((bf16[8,512]{1,0:T(8,128)(2,1)S(1)}, bf16[8,512]{1,0:T(8,128)(2,1)S(1)}, u32[]{:S(2)}, u32[]{:S(2)}) %collective-permute-start) | collective-permute-done | bytes 8224 | tf_op jit(solution)/shard_map/ppermute | solution.py:35
  554.5 19.5 %collective-permute-done.1 = bf16[8,512]{1,0:T(8,128)(2,1)S(1)} collective-permute-done((bf16[8,512]{1,0:T(8,128)(2,1)S(1)}, bf16[8,512]{1,0:T(8,128)(2,1)S(1)}, u32[]{:S(2)}, u32[]{:S(2)}) %collective-permute-start.1) | collective-permute-done | bytes 8224 | tf_op jit(solution)/shard_map/ppermute | solution.py:37
  574.7 2.1 fusion.30
  577.0 3.8 fusion.76
  580.8 4.2 reshape.152
  585.1 11.2 %copy.22 = bf16[20,512,1,2,64]{1,4,3,2,0:T(8,128)(2,1)} copy(bf16[20,512,1,2,64]{4,3,1,0,2:T(2,128)(2,1)} %reshape.152) | data formatting | bytes 5242880
  596.2 90.9 %while.15 = (s32[]{:T(128)}, f32[1,4,2,160]{3,1,2,0:T(4,128)S(1)}, f32[1,4,2,160]{3,1,2,0:T(4,128)}, f32[1,4,2,160,128]{4,3,2,1,0:T(8,128)S(1)}, bf16[20,512,1,2...) while((s32[]{:T(128)}, f32[1,4,2,160]{3,1,2,0:T(4,128)S(1)}, ...), condition=%wide.region_4.5_spmd.clone, body=%wide.region_1.4_spmd.clone.sunk | while | flops 256089600 | bytes 9730209 | solution.py:149
  600.7 1.6 bitcast_reduce_fusion.2
  605.3 1.6 bitcast_reduce_fusion.2
  609.8 1.6 bitcast_reduce_fusion.2
  618.9 1.6 bitcast_reduce_fusion.2
  623.5 1.6 bitcast_reduce_fusion.2
  628.0 1.6 bitcast_reduce_fusion.2
  632.6 1.6 bitcast_reduce_fusion.2
  637.1 1.6 bitcast_reduce_fusion.2
  641.7 1.6 bitcast_reduce_fusion.2
  646.2 1.6 bitcast_reduce_fusion.2
  650.7 1.6 bitcast_reduce_fusion.2
  655.3 1.6 bitcast_reduce_fusion.2
  659.8 1.6 bitcast_reduce_fusion.2
  664.4 1.6 bitcast_reduce_fusion.2
  668.9 1.6 bitcast_reduce_fusion.2
  673.5 1.6 bitcast_reduce_fusion.2
  690.1 2.4 fusion.23
  692.5 4.5 fusion.21
  697.0 3.6 all-to-all-start.1
  701.2 7.0 all-to-all-done.1
  (249 shorter events, 76.9 us)
Async XLA Ops:
  7.2 168.7 %copy-start.7 = (bf16[512,32]{0,1:T(8,128)(2,1)S(1)}, bf16[512,32]{0,1:T(8,128)(2,1)}, u32[]{:S(2)}) copy-start(bf16[512,32]{0,1:T(8,128)(2,1)} %param.18) | copy-start | bytes 98308
  7.2 168.7 %copy-start.6 = (bf16[512,32]{0,1:T(8,128)(2,1)S(1)}, bf16[512,32]{0,1:T(8,128)(2,1)}, u32[]{:S(2)}) copy-start(bf16[512,32]{0,1:T(8,128)(2,1)} %param.19) | copy-start | bytes 98308
  7.2 165.2 %all-gather.3.cloned.1.call-start = ((), (), s32[]{:S(2)}) async-start(), calls=%async_computation.2 | async-start | bytes 3194880 | tf_op jit(solution)/shard_map/all_gather | solution.py:46
  8.7 568.3 %all-gather.5.cloned.1.call-start = ((), (), s32[]{:S(2)}) async-start(), calls=%async_computation.3 | async-start | bytes 5324800 | tf_op jit(solution)/shard_map/all_gather | solution.py:46
  178.5 511.5 %all-to-all-start = ((bf16[64,32,1024]{2,1,0:T(8,128)(2,1)}), bf16[64,32,1024]{2,1,0:T(8,128)(2,1)}, u32[]{:S(2)}, u32[]{:S(2)}) async-start(bf16[64,32,1024]{2,1,0:T(8,128)(2,1)} %stack.2), calls=%async_computation | async-start | bytes 8388608 | tf_op jit(solution)/shard_map/all_to_all | solution.py:16
  192.4 362.2 %collective-permute-start = (bf16[8,512]{1,0:T(8,128)(2,1)S(1)}, bf16[8,512]{1,0:T(8,128)(2,1)S(1)}, u32[]{:S(2)}, u32[]{:S(2)}) collective-permute-start(bf16[8,512]{1,0:T(8,128)(2,1)S(1)} %get-tuple-element.104), channel_id=1, source_target_pairs={{0,4},{4,8},{8,12},{12,16},{16,20},{20,24},{24,28},{28,32},{32,36}... | collective-permute-start | bytes 24584 | tf_op jit(solution)/shard_map/ppermute | solution.py:35
  196.0 378.1 %collective-permute-start.1 = (bf16[8,512]{1,0:T(8,128)(2,1)S(1)}, bf16[8,512]{1,0:T(8,128)(2,1)S(1)}, u32[]{:S(2)}, u32[]{:S(2)}) collective-permute-start(bf16[8,512]{1,0:T(8,128)(2,1)S(1)} %get-tuple-element.105), channel_id=1, source_target_pairs={{4,0},{8,4},{12,8},{16,12},{20,16},{24,20},{28,24},{32,28},{36,32}... | collective-permute-start | bytes 24584 | tf_op jit(solution)/shard_map/ppermute | solution.py:37
  198.0 379.0 %copy-start = (bf16[160,512]{1,0:T(8,128)(2,1)}, bf16[160,512]{1,0:T(8,128)(2,1)S(1)}, u32[]{:S(2)}) copy-start(bf16[160,512]{1,0:T(8,128)(2,1)S(1)} %constant_dynamic-slice_fusion.1) | copy-start | bytes 491524
  597.9 2.2 copy-start.2
  602.4 2.2 copy-start.2
  611.5 2.3 copy-start.2
  616.0 2.3 copy-start.2
  620.6 2.3 copy-start.2
  625.1 2.3 copy-start.2
  629.7 2.3 copy-start.2
  634.2 2.3 copy-start.2
  638.8 2.3 copy-start.2
  643.3 2.3 copy-start.2
  647.9 2.3 copy-start.2
  652.4 2.3 copy-start.2
  657.0 2.3 copy-start.2
  661.5 2.3 copy-start.2
  666.0 2.3 copy-start.2
  670.6 2.3 copy-start.2
  675.1 2.3 copy-start.2
  679.7 2.3 copy-start.2
  684.2 2.3 copy-start.2
  688.1 4.4 copy-start.1
  688.1 4.4 copy-start.5
  688.1 4.4 copy-start.8
  692.5 8.1 %copy-start.4 = (f32[1,4,2,160]{3,1,2,0:T(4,128)S(1)}, f32[1,4,2,160]{3,1,2,0:T(4,128)}, u32[]{:S(2)}) copy-start(f32[1,4,2,160]{3,1,2,0:T(4,128)} %get-tuple-element.42) | copy-start | bytes 15364
  697.0 11.2 %all-to-all-start.1 = ((bf16[4,40,2048]{2,1,0:T(8,128)(2,1)}), bf16[4,40,2048]{2,1,0:T(8,128)(2,1)S(1)}, u32[]{:S(2)}, u32[]{:S(2)}) async-start(bf16[4,40,2048]{2,1,0:T(8,128)(2,1)} %bitcast.10), calls=%async_computation.1 | async-start | bytes 1310720 | tf_op jit(solution)/shard_map/all_to_all | solution.py:74
  (21 other events, 14.3 us)
Sparse Core Ops, SparseCore 0:
  10.7 161.6 all-gather.2
  176.0 311.4 all-gather.4
